TPU v7x, 32 devices: a whole 2x2x4 slice. The times are simulated.
32 devices in a mesh: grp: 2 (over y), fs: 4 (over z), tp: 4 (over x, core).
Axes of the slice: x: 2, y: 2, z: 4, core: 2. Of those that a mesh axis runs over, the one named last changes fastest.
Arguments:
- tokens: bfloat16 [8, 1024, 2048], P(('grp', 'fs'), None, 'tp'), parts along dimension 0, may hold values from -6 to 6
- mix_gain: float32 [2048], replicated, may hold values from 0.1 to 1.9
- in_matrix: float32 [2048, 1024], P('fs', 'tp'), may hold values from -0.125 to 0.125
- in_scale: float32 [1, 1024], P(None, 'tp'), may hold values from 0.5 to 2
- pool_mix: bfloat16 [8, 128, 128], P('tp'), may hold values from -0.5 to 0.5
- pool_scale: float32 [1, 1024], P(None, 'tp'), may hold values from 0.1 to 1.9
- out_matrix: float32 [1024, 2048], P('tp', 'fs'), may hold values from -0.25 to 0.25
- out_scale: float32 [1, 2048], P(None, 'fs'), may hold values from 0.5 to 2
- ffn_gain: float32 [2048], replicated, may hold values from 0.1 to 1.9
- gate_matrix: float32 [2048, 5632], P('fs', 'tp'), may hold values from -0.125 to 0.125
- gate_scale: float32 [1, 5632], P(None, 'tp'), may hold values from 0.5 to 2
- up_matrix: float32 [2048, 5632], P('fs', 'tp'), may hold values from -0.125 to 0.125
- up_scale: float32 [1, 5632], P(None, 'tp'), may hold values from 0.5 to 2
- gate_taps: float32 [3, 5632], P(None, 'tp'), may hold values from -4 to 4
- up_taps: float32 [3, 5632], P(None, 'tp'), may hold values from -4 to 4
- down_matrix: float32 [5632, 2048], P('tp', 'fs'), may hold values from -0.109375 to 0.109375
- down_scale: float32 [1, 2048], P(None, 'fs'), may hold values from 0.5 to 2
Outputs:
- layer_out: bfloat16 [8, 1024, 2048], P(('grp', 'fs'), None, 'tp'), parts along dimension 0
There are 2 independent parts, one for each index of `grp`. A program takes and returns all parts, laid end to end along the dimension named above; an argument that names none is the same for every part. Nothing has to cross between parts.
All inputs are finite; a program needn't handle non-finite values.
Results may differ from a plain program's by a relative error of at most 0.025.
Values may be sent and summed in bfloat16 or wider, within the bound.
No kernel may reach another device: no remote copies, remote signals or barrier semaphores. Data moves between devices by JAX's collectives and lax.ppermute only.
A program may use at most 128 MiB of HBM per device.

v0:
```python
import jax
import jax.numpy as jnp
from jax import lax
from jax.sharding import PartitionSpec as P

BLOCKS = 8


eps = 1e-06
widest_span = 16


def norm_rows(tok_rows, norm_gain):
    values = tok_rows.astype(jnp.float32)
    scaled = values * lax.rsqrt(jnp.mean(values * values, axis=-1, keepdims=True) + eps)
    return (scaled * norm_gain).astype(jnp.bfloat16)


def span_widths(block_ids):
    return jnp.left_shift(jnp.ones_like(block_ids), 1 + 4 * block_ids // BLOCKS)


def trailing_gap(projected, windows):
    values = projected.astype(jnp.float32)
    length = values.shape[0]
    running = values
    for offset in range(1, widest_span):
        shifted = jnp.pad(values[: length - offset], ((offset, 0), (0, 0)))
        running = running + jnp.where(windows[None, :] > offset, shifted, jnp.zeros_like(shifted))
    positions = jnp.arange(length, dtype=jnp.int32)[:, None]
    counts = jnp.minimum(positions + 1, windows[None, :]).astype(jnp.float32)
    return (running / counts - values).astype(jnp.bfloat16)


def causal_taps(linear, tap_table):
    values = linear.astype(jnp.float32)
    length = values.shape[0]
    back_one = jnp.pad(values[: length - 1], ((1, 0), (0, 0)))
    back_two = jnp.pad(values[: length - 2], ((2, 0), (0, 0)))
    return tap_table[2] * values + tap_table[1] * back_one + tap_table[0] * back_two


def fold_rows(operand, portion):
    return jnp.dot(operand, portion, preferred_element_type=jnp.float32)


def shards(
    tokens,
    mix_gain,
    in_matrix,
    in_scale,
    pool_mix,
    pool_scale,
    out_matrix,
    out_scale,
    ffn_gain,
    gate_matrix,
    gate_scale,
    up_matrix,
    up_scale,
    gate_taps,
    up_taps,
    down_matrix,
    down_scale,
):
    length = tokens.shape[1]
    own_width = tokens.shape[2]
    local_rows = tokens.reshape(length, own_width)
    gathered = lax.all_gather(local_rows, "tp", axis=1, tiled=True)
    normed = norm_rows(gathered, mix_gain)
    width_in = in_matrix.shape[1]
    in_total = fold_rows(
        normed, lax.all_gather(in_matrix.astype(jnp.bfloat16), "fs", axis=0, tiled=True)
    )
    projected = (in_total * in_scale).astype(jnp.bfloat16)
    local_blocks = pool_mix.shape[0]
    block_width = pool_mix.shape[1]
    block_ids = lax.axis_index("tp") * local_blocks + jnp.arange(local_blocks, dtype=jnp.int32)
    windows = jnp.repeat(span_widths(block_ids), block_width)
    spread = trailing_gap(projected, windows)
    block_mixed = jnp.einsum(
        "lbc,bce->lbe",
        spread.reshape(length, local_blocks, block_width),
        pool_mix,
        preferred_element_type=jnp.float32,
    ).reshape(length, width_in)
    pooled = (block_mixed * pool_scale).astype(jnp.bfloat16)
    out_cols = lax.all_gather(out_scale, "fs", axis=1, tiled=True)
    tp_index = lax.axis_index("tp")
    groups = lax.axis_size("tp")
    pooled_all = lax.all_gather(pooled, "tp", axis=1, tiled=True)
    row_block = lax.all_gather(out_matrix.astype(jnp.bfloat16), "fs", axis=1, tiled=True)
    own_matrix = lax.all_to_all(row_block, "tp", split_axis=1, concat_axis=0, tiled=True)
    own_scales = lax.dynamic_slice_in_dim(out_cols, tp_index * own_width, own_width, 1)
    grouped_rows = pooled_all.reshape(length, groups, width_in)
    grouped_matrix = own_matrix.reshape(groups, width_in, own_width)
    pieces = (
        jnp.einsum("lgc,gcd->gld", grouped_rows, grouped_matrix, preferred_element_type=jnp.float32)
        * own_scales[None]
    )
    rounded = lax.optimization_barrier(pieces.astype(jnp.bfloat16))
    mixing = jnp.sum(rounded.astype(jnp.float32), axis=0)
    residual = (local_rows.astype(jnp.float32) + mixing).astype(jnp.bfloat16)
    gathered_ffn = lax.all_gather(residual, "tp", axis=1, tiled=True)
    normed_ffn = norm_rows(gathered_ffn, ffn_gain)
    gate_cast = gate_matrix.astype(jnp.bfloat16)
    up_cast = up_matrix.astype(jnp.bfloat16)
    gate_full, up_full = (
        lax.all_gather(gate_cast, "fs", axis=0, tiled=True),
        lax.all_gather(up_cast, "fs", axis=0, tiled=True),
    )
    gate_total = jnp.dot(normed_ffn, gate_full, preferred_element_type=jnp.float32)
    up_total = jnp.dot(normed_ffn, up_full, preferred_element_type=jnp.float32)
    gate_lin = (gate_total * gate_scale).astype(jnp.bfloat16)
    up_lin = (up_total * up_scale).astype(jnp.bfloat16)
    hidden = (jax.nn.silu(causal_taps(gate_lin, gate_taps)) * causal_taps(up_lin, up_taps)).astype(
        jnp.bfloat16
    )
    down_cols = lax.all_gather(down_scale, "fs", axis=1, tiled=True)
    partial_ffn = (
        jnp.dot(
            hidden,
            lax.all_gather(down_matrix.astype(jnp.bfloat16), "fs", axis=1, tiled=True),
            preferred_element_type=jnp.float32,
        )
        * down_cols
    )
    feed_out = lax.psum_scatter(
        partial_ffn.astype(jnp.bfloat16), "tp", scatter_dimension=1, tiled=True
    ).astype(jnp.float32)
    result = (residual.astype(jnp.float32) + feed_out).astype(jnp.bfloat16)
    return result.reshape(1, length, result.shape[1])


def solution(mesh):
    return jax.shard_map(
        shards,
        mesh=mesh,
        in_specs=(
            P(("grp", "fs"), None, "tp"),
            P(),
            P("fs", "tp"),
            P(None, "tp"),
            P("tp", None, None),
            P(None, "tp"),
            P("tp", "fs"),
            P(None, "fs"),
            P(),
            P("fs", "tp"),
            P(None, "tp"),
            P("fs", "tp"),
            P(None, "tp"),
            P(None, "tp"),
            P(None, "tp"),
            P("tp", "fs"),
            P(None, "fs"),
        ),
        out_specs=P(("grp", "fs"), None, "tp"),
        check_vma=False,
    )
```

profile of v0, /device:TPU:0, one launch (start us, length us, event | category | flops | bytes accessed | tf_op | source)
XLA Modules:
  0.0 573.4 jit_solution(17679194408588764987)
XLA Ops:
  6.5 0.7 all-gather.24.cloned.1.call-update
  7.3 0.0 all-gather.10.cloned.1.call-start
  7.3 1.8 convert_element_type.120
  9.1 0.0 all-gather.10.cloned.1.call-update
  9.1 0.0 all-gather.14.cloned.1.call-start
  9.2 1.9 copy.22
  11.0 0.0 all-gather.14.cloned.1.call-update
  11.1 0.0 all-gather.12.cloned.1.call-start
  11.1 0.1 bitcast_compare_fusion.14
  11.2 0.1 broadcast_bitcast_fusion
  11.3 34.8 %all-gather.24.cloned.1.call-done = bf16[1,1024,2048]{2,1,0:T(8,128)(2,1)} async-done(((bf16[1,1024,512]{2,1,0:T(8,128)(2,1)}), bf16[1,1024,2048]{2,1,0:T(8,128)(2,1)}) %all-gather.24.cloned.1.call-update) | async-done | bytes 4194320 | tf_op jit(solution)/shard_map/all_gather | solution.py:69
  46.1 3.1 fusion.3
  49.2 26.5 %all-gather.10.cloned.1.call-done = bf16[2048,256]{1,0:T(8,128)(2,1)} async-done(((bf16[512,256]{1,0:T(8,128)(2,1)}), bf16[2048,256]{1,0:T(8,128)(2,1)}) %all-gather.10.cloned.1.call-update) | async-done | bytes 1048592 | tf_op jit(solution)/shard_map/all_gather | solution.py:73
  75.7 3.8 fusion.20
  79.5 0.1 slice.107
  79.6 0.1 slice.108
  79.7 0.1 slice.109
  79.7 0.1 slice.110
  79.8 0.1 slice.111
  79.9 0.1 slice.112
  80.0 0.1 slice.113
  80.0 0.1 slice.114
  80.1 0.0 copy-start.12
  80.1 3.2 fusion.28
  83.4 0.9 fusion.26
  84.3 0.0 all-gather.12.cloned.1.call-update
  84.3 20.3 %all-gather.14.cloned.1.call-done = bf16[256,2048]{0,1:T(8,128)(2,1)} async-done(((bf16[256,512]{0,1:T(8,128)(2,1)}), bf16[256,2048]{0,1:T(8,128)(2,1)}) %all-gather.14.cloned.1.call-update) | async-done | bytes 1048592 | tf_op jit(solution)/shard_map/all_gather | solution.py:92
  104.7 2.3 copy.23
  106.9 3.5 all-to-all-start
  110.5 0.0 all-gather.16.cloned.1.call-start
  110.5 11.9 %all_gather.34 = f32[1,2048]{1,0:T(1,128)S(1)} all-gather(f32[1,512]{1,0:T(1,128)S(1)} %copy-done.10), channel_id=1, replica_groups=mesh['grp'=2,'fs'=4,'tp'=4] {'fs'}, dimensions={1}, use_global_device_ids=true | all-gather | bytes 10240 | tf_op jit(solution)/shard_map/all_gather | solution.py:88
  122.5 12.5 %all-to-all-done = bf16[256,4,512]{2,0,1:T(8,128)(2,1)S(1)} async-done(((bf16[256,4,512]{2,0,1:T(8,128)(2,1)}), bf16[256,4,512]{2,0,1:T(8,128)(2,1)S(1)}, u32[]{:S(2)}, u32[]{:S(2)}) %all-to-all-start) | async-done | bytes 1048608 | tf_op jit(solution)/shard_map/all_to_all | solution.py:93
  135.0 2.7 all-gather.12.cloned.1.call-done
  137.6 3.0 multiply_convert_fusion.1
  140.6 0.0 copy-start.4
  140.6 0.7 convert_reduce_fusion
  141.3 1.3 fusion.13
  142.6 0.0 all-gather.16.cloned.1.call-update
  142.7 0.0 all-gather.18.cloned.1.call-start
  142.7 1.3 convert_element_type.133
  144.0 0.0 all-gather.18.cloned.1.call-update
  144.1 0.0 copy-start.8
  144.1 0.0 copy-start.9
  144.1 0.0 copy-start.7
  144.1 0.0 all-gather.20.cloned.1.call-start
  144.2 3.3 convert_element_type.136
  147.5 0.0 all-gather.20.cloned.1.call-update
  147.5 0.0 all-gather.22.cloned.1.call-start
  147.5 1.3 convert_element_type.140
  148.8 0.0 all-gather.22.cloned.1.call-update
  148.8 0.0 reduce-scatter.2.cloned.1.call-start
  149.0 12.1 %all_gather.39 = f32[1,2048]{1,0:T(1,128)S(1)} all-gather(f32[1,512]{1,0:T(1,128)S(1)} %copy-done.11), channel_id=1, replica_groups=mesh['grp'=2,'fs'=4,'tp'=4] {'fs'}, dimensions={1}, use_global_device_ids=true | all-gather | bytes 10240 | tf_op jit(solution)/shard_map/all_gather | solution.py:119
  161.1 0.1 slice_reduce_fusion.2
  161.2 14.5 %all-gather.16.cloned.1.call-done = bf16[1024,2048]{1,0:T(8,128)(2,1)} async-done(((bf16[1024,512]{1,0:T(8,128)(2,1)}), bf16[1024,2048]{1,0:T(8,128)(2,1)}) %all-gather.16.cloned.1.call-update) | async-done | bytes 4194320 | tf_op jit(solution)/shard_map/all_gather | solution.py:104
  175.7 3.1 fusion
  178.8 105.1 %all-gather.18.cloned.1.call-done = bf16[2048,1408]{1,0:T(8,128)(2,1)} async-done(((bf16[512,1408]{1,0:T(8,128)(2,1)}), bf16[2048,1408]{1,0:T(8,128)(2,1)}) %all-gather.18.cloned.1.call-update) | async-done | bytes 5767184 | tf_op jit(solution)/shard_map/all_gather | solution.py:109
  283.9 11.9 %fusion.11 = f32[1024,1408]{1,0:T(8,128)} fusion(bf16[2048,1408]{1,0:T(8,128)(2,1)} %all-gather.18.cloned.1.call-done, f32[1408]{0:T(1024)S(1)} %reduce.1, bf16[1024,2048]{1,0:T(8,128)(2,1)} %all-gather.16.cloned.1.call-done, f32[2048]{0:T(1024)S(1)} %copy-done.14, f32[1024]{0:T(1024)S(1)} %add_rsqrt_fusion), kind=kOutput, calls=%fused_computation.20 | convolution fusion | flops 5918294016 | bytes 15746560 | tf_op jit(solution)/shard_map/dot_general | solution.py:112
  295.8 94.7 %all-gather.20.cloned.1.call-done = bf16[2048,1408]{1,0:T(8,128)(2,1)} async-done(((bf16[512,1408]{1,0:T(8,128)(2,1)}), bf16[2048,1408]{1,0:T(8,128)(2,1)}) %all-gather.20.cloned.1.call-update) | async-done | bytes 5767184 | tf_op jit(solution)/shard_map/all_gather | solution.py:110
  390.4 12.0 %fusion.12 = f32[1024,1408]{1,0:T(8,128)} fusion(bf16[2048,1408]{1,0:T(8,128)(2,1)} %all-gather.20.cloned.1.call-done, f32[1408]{0:T(1024)S(1)} %reduce.5, bf16[1024,2048]{1,0:T(8,128)(2,1)} %all-gather.16.cloned.1.call-done, f32[2048]{0:T(1024)S(1)} %copy-done.14, f32[1024]{0:T(1024)S(1)} %add_rsqrt_fusion), kind=kOutput, calls=%fused_computation.21 | convolution fusion | flops 5918294016 | bytes 15746560 | tf_op jit(solution)/shard_map/dot_general | solution.py:113
  402.4 94.6 %all-gather.22.cloned.1.call-done = bf16[1408,2048]{1,0:T(8,128)(2,1)} async-done(((bf16[1408,512]{1,0:T(8,128)(2,1)}), bf16[1408,2048]{1,0:T(8,128)(2,1)}) %all-gather.22.cloned.1.call-update) | async-done | bytes 5767184 | tf_op jit(solution)/shard_map/all_gather | solution.py:123
  497.0 24.6 %multiply_convert_fusion = bf16[1024,2048]{1,0:T(8,128)(2,1)} fusion(bf16[1408,2048]{1,0:T(8,128)(2,1)} %all-gather.22.cloned.1.call-done, f32[2048]{0:T(1024)S(1)} %bitcast.83, f32[1022,1408]{1,0:T(8,128)} %bitcast.89, f32[1023,1408]{1,0:T(8,128)} %bitcast.90, f32[1024,1408]{1,0:T(8,128)} %fusion.12, f32[1022,1408]{1,0:T(8,128)} %bitcast.87, ...), kind=kOutput, calls=%fused_computation.10 | convolution fusion | flops 5932843008 | bytes 44572672 | tf_op jit(solution)/shard_map/dot_general | solution.py:121
  521.6 0.0 reduce-scatter.2.cloned.1.call-update
  521.6 42.8 %reduce-scatter.2.cloned.1.call-done = bf16[1024,512]{1,0:T(8,128)(2,1)} async-done(((bf16[1024,2048]{1,0:T(8,128)(2,1)}), bf16[1024,512]{1,0:T(8,128)(2,1)}) %reduce-scatter.2.cloned.1.call-update) | async-done | bytes 1048592 | tf_op jit(solution)/shard_map/reduce_scatter | solution.py:128
  564.4 2.5 fusion.25
  (35 shorter events, 0.1 us)
Async XLA Ops:
  6.5 73.6 %copy-start = (bf16[2,128,128]{2,1,0:T(8,128)(2,1)S(1)}, bf16[2,128,128]{2,1,0:T(8,128)(2,1)}, u32[]{:S(2)}) copy-start(bf16[2,128,128]{2,1,0:T(8,128)(2,1)} %param.21) | copy-start | bytes 196612
  6.5 69.2 %copy-start.15 = (f32[1,256]{1,0:T(1,128)S(1)}, f32[1,256]{1,0:T(1,128)}, u32[]{:S(2)}) copy-start(f32[1,256]{1,0:T(1,128)} %param.20) | copy-start | bytes 3076
  6.5 69.2 %copy-start.13 = (f32[2048]{0:T(1024)S(1)}, f32[2048]{0:T(1024)}, u32[]{:S(2)}) copy-start(f32[2048]{0:T(1024)} %param.18) | copy-start | bytes 24580
  6.5 39.6 %all-gather.24.cloned.1.call-start = ((), (), s32[]{:S(2)}) async-start(), calls=%async_computation.10 | async-start | bytes 5242880 | tf_op jit(solution)/shard_map/all_gather | solution.py:69
  7.3 68.4 %all-gather.10.cloned.1.call-start = ((), (), s32[]{:S(2)}) async-start(), calls=%async_computation.2 | async-start | bytes 1310720 | tf_op jit(solution)/shard_map/all_gather | solution.py:73
  9.1 95.6 %all-gather.14.cloned.1.call-start = ((), (), s32[]{:S(2)}) async-start(), calls=%async_computation.4 | async-start | bytes 1310720 | tf_op jit(solution)/shard_map/all_gather | solution.py:92
  11.1 126.6 %all-gather.12.cloned.1.call-start = ((), (), s32[]{:S(2)}) async-start(), calls=%async_computation.3 | async-start | bytes 2621440 | tf_op jit(solution)/shard_map/all_gather | solution.py:91
  80.1 3.3 copy-start.12
  83.4 27.1 %copy-start.10 = (f32[1,512]{1,0:T(1,128)S(1)}, f32[1,512]{1,0:T(1,128)}, u32[]{:S(2)}) copy-start(f32[1,512]{1,0:T(1,128)} %param.24) | copy-start | bytes 6148
  106.9 28.0 %all-to-all-start = ((bf16[256,4,512]{2,0,1:T(8,128)(2,1)}), bf16[256,4,512]{2,0,1:T(8,128)(2,1)S(1)}, u32[]{:S(2)}, u32[]{:S(2)}) async-start(bf16[256,4,512]{2,0,1:T(8,128)(2,1)} %copy.23), calls=%async_computation | async-start | bytes 2097152 | tf_op jit(solution)/shard_map/all_to_all | solution.py:93
  110.5 65.3 %all-gather.16.cloned.1.call-start = ((), (), s32[]{:S(2)}) async-start(), calls=%async_computation.5 | async-start | bytes 5242880 | tf_op jit(solution)/shard_map/all_gather | solution.py:104
  137.6 3.7 copy-start.3
  140.6 2.1 copy-start.4
  142.7 141.2 %all-gather.18.cloned.1.call-start = ((), (), s32[]{:S(2)}) async-start(), calls=%async_computation.6 | async-start | bytes 7208960 | tf_op jit(solution)/shard_map/all_gather | solution.py:109
  144.0 3.5 copy-start.5
  144.1 4.8 copy-start.8
  144.1 4.9 copy-start.9
  144.1 4.9 copy-start.11
  144.1 17.0 %copy-start.6 = (f32[3,1408]{1,0:T(4,128)S(1)}, f32[3,1408]{1,0:T(4,128)}, u32[]{:S(2)}) copy-start(f32[3,1408]{1,0:T(4,128)} %param.31) | copy-start | bytes 50692
  144.1 17.0 %copy-start.7 = (f32[3,1408]{1,0:T(4,128)S(1)}, f32[3,1408]{1,0:T(4,128)}, u32[]{:S(2)}) copy-start(f32[3,1408]{1,0:T(4,128)} %param.30) | copy-start | bytes 50692
  144.1 246.3 %all-gather.20.cloned.1.call-start = ((), (), s32[]{:S(2)}) async-start(), calls=%async_computation.7 | async-start | bytes 7208960 | tf_op jit(solution)/shard_map/all_gather | solution.py:110
  147.5 136.4 %copy-start.14 = (f32[2048]{0:T(1024)S(1)}, f32[2048]{0:T(1024)}, u32[]{:S(2)}) copy-start(f32[2048]{0:T(1024)} %param.25) | copy-start | bytes 24580
  147.5 349.5 %all-gather.22.cloned.1.call-start = ((), (), s32[]{:S(2)}) async-start(), calls=%async_computation.8 | async-start | bytes 7208960 | tf_op jit(solution)/shard_map/all_gather | solution.py:123
  148.8 415.6 %reduce-scatter.2.cloned.1.call-start = ((), (), s32[]{:S(2)}) async-start(), calls=%async_computation.9 | async-start | bytes 5242880 | tf_op jit(solution)/shard_map/reduce_scatter | solution.py:128
  497.0 67.4 %copy-start.2 = (bf16[1024,512]{1,0:T(8,128)(2,1)S(1)}, bf16[1024,512]{1,0:T(8,128)(2,1)}, u32[]{:S(2)}) copy-start(bf16[1024,512]{1,0:T(8,128)(2,1)} %fusion.13) | copy-start | bytes 3145732
  497.0 69.9 %copy-start.1 = (bf16[2,128,128]{2,1,0:T(8,128)(2,1)S(1)}, bf16[2,128,128]{2,1,0:T(8,128)(2,1)}, u32[]{:S(2)}) copy-start(bf16[2,128,128]{2,1,0:T(8,128)(2,1)} %param.21) | copy-start | bytes 196612
Sparse Core Ops, SparseCore 0:
  8.9 37.1 all-gather.23
  47.7 27.9 all-gather.9
  77.3 27.3 all-gather.13
  106.1 31.4 all-gather.11
  142.8 32.9 all-gather.15
  177.2 106.6 all-gather.17
  285.5 104.9 all-gather.19
  392.0 104.9 all-gather.21
  521.8 42.6 reduce-scatter.1
where the time goes:
time: 574 us; the launch traced here: 573 us
  waiting for transfers between devices  449 us (78%)
  matrix products  58.5 us (10%)
  blocking collectives  24.1 us (4%)
  other arithmetic  19.3 us (3%)
  between operations  13.5 us (2%)
    all_gather x1, waiting for transfers between devices, shards(): lax.all_gather(gate_cast, 'fs', axis=0, tiled=True)  105 us
    all_gather x1, waiting for transfers between devices, shards(): lax.all_gather(up_cast, 'fs', axis=0, tiled=True)  94.7 us
    all_gather x1, waiting for transfers between devices, shards(): lax.all_gather(down_matrix.astype(jnp.bfloat16), 'fs', axis=1, tiled=True)  94.6 us
    reduce_scatter x1, waiting for transfers between devices, shards(): lax.psum_scatter(partial_ffn.astype(jnp.bfloat16), 'tp', scatter_dimensio...  42.8 us
    all_gather x1, waiting for transfers between devices, shards(): gathered = lax.all_gather(local_rows, 'tp', axis=1, tiled=True)  34.8 us
    all_gather x1, waiting for transfers between devices, shards(): lax.all_gather(in_matrix.astype(jnp.bfloat16), 'fs', axis=0, tiled=True)  26.5 us
    dot_general x1, matrix products, shards(): jnp.dot(hidden, lax.all_gather(down_matrix.astype(jnp.bfloat16), 'fs', ax...  24.6 us
    all_gather x1, waiting for transfers between devices, shards(): lax.all_gather(out_matrix.astype(jnp.bfloat16), 'fs', axis=1, tiled=True)  20.3 us
  transfers between devices with their start and end apart: 10, of which 10 were waited for; matrix products, arithmetic and copies ran while one was open for 9% of the time, Pallas kernels for 0%

commit v1 on v0

v1 whole, which is shorter than its diff:
```python
import jax
import jax.numpy as jnp
from jax import lax
from jax.sharding import PartitionSpec as P

BLOCKS = 8


eps = 1e-06
widest_span = 16


def norm_rows(tok_rows, norm_gain):
    values = tok_rows.astype(jnp.float32)
    scaled = values * lax.rsqrt(jnp.mean(values * values, axis=-1, keepdims=True) + eps)
    return (scaled * norm_gain).astype(jnp.bfloat16)


def span_widths(block_ids):
    return jnp.left_shift(jnp.ones_like(block_ids), 1 + 4 * block_ids // BLOCKS)


def trailing_gap(projected, windows):
    values = projected.astype(jnp.float32)
    length = values.shape[0]
    running = values
    for offset in range(1, widest_span):
        shifted = jnp.pad(values[: length - offset], ((offset, 0), (0, 0)))
        running = running + jnp.where(windows[None, :] > offset, shifted, jnp.zeros_like(shifted))
    positions = jnp.arange(length, dtype=jnp.int32)[:, None]
    counts = jnp.minimum(positions + 1, windows[None, :]).astype(jnp.float32)
    return (running / counts - values).astype(jnp.bfloat16)


def causal_taps(linear, tap_table):
    values = linear.astype(jnp.float32)
    length = values.shape[0]
    back_one = jnp.pad(values[: length - 1], ((1, 0), (0, 0)))
    back_two = jnp.pad(values[: length - 2], ((2, 0), (0, 0)))
    return tap_table[2] * values + tap_table[1] * back_one + tap_table[0] * back_two


def fold_rows(operand, portion):
    return jnp.dot(operand, portion, preferred_element_type=jnp.float32)


def tp_swap(value):
    size = lax.axis_size("tp")
    return lax.ppermute(value, "tp", [(i, i ^ 1) for i in range(size)])


def tp_step(value, step):
    size = lax.axis_size("tp")
    chips = size // 2
    pairs = [(i, ((i // 2 + step) % chips) * 2 + i % 2) for i in range(size)]
    return lax.ppermute(value, "tp", pairs)


def tp_pieces(value):
    chips = lax.axis_size("tp") // 2
    near = [value] + [tp_step(value, step) for step in range(1, chips)]
    pieces = []
    for piece in near:
        pieces += [piece, tp_swap(piece)]
    return pieces


def tp_sources():
    chips = lax.axis_size("tp") // 2
    index = lax.axis_index("tp")
    ids = []
    for step in range(chips):
        chip = (index // 2 + chips - step) % chips
        ids += [chip * 2 + index % 2, chip * 2 + 1 - index % 2]
    return ids


def pick_blocks(array, ids, axis=0):
    width = array.shape[axis] // len(ids)
    return jnp.concatenate(
        [lax.dynamic_slice_in_dim(array, i * width, width, axis) for i in ids], axis
    )


def part_columns(array, which, parts):
    width = array.shape[1] // parts
    chosen = array[:, :width]
    for i in range(1, parts):
        chosen = jnp.where(which == i, array[:, i * width : (i + 1) * width], chosen)
    return chosen


def column_block(stacked, index, blocks):
    count, rows, width = stacked.shape
    if count % blocks == 0:
        n = count // blocks
        taken = lax.dynamic_slice_in_dim(stacked, index * n, n, 0)
        return jnp.moveaxis(taken, 0, 1).reshape(rows, n * width)
    whole = jnp.moveaxis(stacked, 0, 1).reshape(rows, count * width)
    own = count * width // blocks
    return lax.dynamic_slice_in_dim(whole, index * own, own, 1)


def shards(
    tokens,
    mix_gain,
    in_matrix,
    in_scale,
    pool_mix,
    pool_scale,
    out_matrix,
    out_scale,
    ffn_gain,
    gate_matrix,
    gate_scale,
    up_matrix,
    up_scale,
    gate_taps,
    up_taps,
    down_matrix,
    down_scale,
):
    length = tokens.shape[1]
    own_width = tokens.shape[2]
    bf16 = jnp.bfloat16
    tp_index = lax.axis_index("tp")
    tp_size = lax.axis_size("tp")
    group = lax.axis_index("grp")
    parts = lax.axis_size("grp")
    ids = tp_sources()
    local_rows = tokens.reshape(length, own_width)
    gathered = jnp.concatenate(tp_pieces(local_rows), axis=1)

    in_full = lax.all_gather(in_matrix.astype(bf16), "fs", axis=0, tiled=True)
    out_rows = lax.all_gather((out_matrix * out_scale).astype(bf16), "fs", axis=1, tiled=True)
    own_matrix = lax.all_to_all(out_rows, "tp", split_axis=1, concat_axis=0, tiled=True)

    def across_groups(held):
        size = parts
        return [held] + [
            lax.ppermute(held, "grp", [(i, (i - step) % size) for i in range(size)])
            for step in range(1, size)
        ]

    gate_part = part_columns(gate_matrix, group, parts).astype(bf16)
    up_part = part_columns(up_matrix, group, parts).astype(bf16)
    down_height = down_matrix.shape[0] // parts
    down_part = lax.dynamic_slice_in_dim(down_matrix, group * down_height, down_height, 0)
    down_part = (down_part * down_scale).astype(bf16)
    gate_parts = across_groups(lax.all_gather(gate_part, "fs", axis=0, tiled=True))
    up_parts = across_groups(lax.all_gather(up_part, "fs", axis=0, tiled=True))
    down_parts = across_groups(lax.all_gather(down_part, "fs", axis=0, tiled=False))

    normed = norm_rows(gathered, pick_blocks(mix_gain, ids))
    width_in = in_matrix.shape[1]
    projected = (fold_rows(normed, pick_blocks(in_full, ids)) * in_scale).astype(bf16)
    local_blocks = pool_mix.shape[0]
    block_width = pool_mix.shape[1]
    block_ids = tp_index * local_blocks + jnp.arange(local_blocks, dtype=jnp.int32)
    windows = jnp.repeat(span_widths(block_ids), block_width)
    spread = trailing_gap(projected, windows)
    block_mixed = jnp.einsum(
        "lbc,bce->lbe",
        spread.reshape(length, local_blocks, block_width),
        pool_mix,
        preferred_element_type=jnp.float32,
    ).reshape(length, width_in)
    pooled = (block_mixed * pool_scale).astype(bf16)
    pooled_all = jnp.concatenate(tp_pieces(pooled), axis=1)
    mixing = fold_rows(pooled_all, pick_blocks(own_matrix, ids))
    residual = (local_rows.astype(jnp.float32) + mixing).astype(bf16)

    gathered_ffn = jnp.concatenate(tp_pieces(residual), axis=1)
    normed_ffn = norm_rows(gathered_ffn, pick_blocks(ffn_gain, ids))
    hidden_parts = []
    for step in range(parts):
        which = (group + step) % parts
        gate_total = fold_rows(normed_ffn, pick_blocks(gate_parts[step], ids))
        up_total = fold_rows(normed_ffn, pick_blocks(up_parts[step], ids))
        gate_lin = (gate_total * part_columns(gate_scale, which, parts)).astype(bf16)
        up_lin = (up_total * part_columns(up_scale, which, parts)).astype(bf16)
        gate_conv = causal_taps(gate_lin, part_columns(gate_taps, which, parts))
        up_conv = causal_taps(up_lin, part_columns(up_taps, which, parts))
        hidden_parts.append((jax.nn.silu(gate_conv) * up_conv).astype(bf16))

    def down_product(index):
        total = None
        for hidden, stacked in zip(hidden_parts, down_parts):
            piece = fold_rows(hidden, column_block(stacked, index, tp_size))
            total = piece if total is None else total + piece
        return total

    chips = tp_size // 2
    chip, core = tp_index // 2, tp_index % 2
    feed_out = jnp.zeros((length, own_width), jnp.float32)
    for step in list(range(1, chips)) + [0]:
        target = (chip + step) % chips
        other = tp_swap(down_product(target * 2 + 1 - core).astype(bf16))
        summed = down_product(target * 2 + core) + other.astype(jnp.float32)
        if step:
            summed = tp_step(summed.astype(bf16), step).astype(jnp.float32)
        feed_out = feed_out + summed
    result = (residual.astype(jnp.float32) + feed_out).astype(bf16)
    return result.reshape(1, length, result.shape[1])


def solution(mesh):
    return jax.shard_map(
        shards,
        mesh=mesh,
        in_specs=(
            P(("grp", "fs"), None, "tp"),
            P(),
            P("fs", "tp"),
            P(None, "tp"),
            P("tp", None, None),
            P(None, "tp"),
            P("tp", "fs"),
            P(None, "fs"),
            P(),
            P("fs", "tp"),
            P(None, "tp"),
            P("fs", "tp"),
            P(None, "tp"),
            P(None, "tp"),
            P(None, "tp"),
            P("tp", "fs"),
            P(None, "fs"),
        ),
        out_specs=P(("grp", "fs"), None, "tp"),
        check_vma=False,
    )
```

time: 574 us -> 380 us (0.66)
  waiting for transfers between devices: 449 us -> 265 us
  blocking collectives: 24.1 us -> 0 us
  matrix products: 58.5 us -> 43.4 us
  starting transfers between devices: 3.85 us -> 16.3 us
  local copies, waits for them, and re-layouts: 4.94 us -> 16.3 us
    all_gather x8 -> x5, waiting for transfers between devices: 393 us -> 139 us  [the longest x1 57.8 us: shards(): up_parts = across_groups(lax.all_gather(up_part, 'fs', axis=0, tiled=True))]
    ppermute x0 -> x15, waiting for transfers between devices: none -> 112 us  [the longest x4 63.4 us: tp_step(): return lax.ppermute(value, 'tp', pairs)]
    dot_general x4 -> x0, matrix products: 51.5 us -> none  [the longest x1 24.6 us: shards(): jnp.dot(hidden, lax.all_gather(down_matrix.astype(jnp.bfloat16), 'fs', ax...]
    reduce_scatter x1 -> x0, waiting for transfers between devices: 42.8 us -> none  [shards(): lax.psum_scatter(partial_ffn.astype(jnp.bfloat16), 'tp', scatter_dimensio...]
    dot_general x1 -> x14, matrix products: 3.8 us -> 40.2 us  [fold_rows(): return jnp.dot(operand, portion, preferred_element_type=jnp.float32)]
    all_gather x2 -> x0, blocking collectives: 24.1 us -> none  [the longest x1 12.1 us: shards(): down_cols = lax.all_gather(down_scale, 'fs', axis=1, tiled=True)]
    ppermute x0 -> x15, starting transfers between devices: none -> 12.4 us  [the longest x4 6.75 us: tp_step(): return lax.ppermute(value, 'tp', pairs)]
    convert_element_type x6 -> x9, other arithmetic: 9.91 us -> 17.9 us  [the longest x2 10 us: shards(): hidden_parts.append((jax.nn.silu(gate_conv) * up_conv).astype(bf16))]
  transfers between devices with their start and end apart: 10 -> 21, of which waited for: 10 -> 10; matrix products, arithmetic and copies ran while one was open for 9% -> 20% of each run, Pallas kernels for 0% -> 0%
where the time goes in v1:
time: 380 us; the launch traced here: 379 us
  waiting for transfers between devices  265 us (70%)
  matrix products  43.4 us (11%)
  other arithmetic  24.9 us (7%)
  local copies, waits for them, and re-layouts  16.3 us (4%)
  starting transfers between devices  16.3 us (4%)
  between operations  13.9 us (4%)
    ppermute x4, waiting for transfers between devices, tp_step(): return lax.ppermute(value, 'tp', pairs)  63.4 us
    all_gather x1, waiting for transfers between devices, shards(): up_parts = across_groups(lax.all_gather(up_part, 'fs', axis=0, tiled=True))  57.8 us
    all_gather x1, waiting for transfers between devices, shards(): lax.all_gather(gate_part, 'fs', axis=0, tiled=True)  57.8 us
    ppermute x3, waiting for transfers between devices, across_groups(): lax.ppermute(held, 'grp', [(i, (i - step) % size) for i in range(size)])  48.4 us
    dot_general x14, matrix products, fold_rows(): return jnp.dot(operand, portion, preferred_element_type=jnp.float32)  40.2 us
    all_to_all x1, waiting for transfers between devices, shards(): lax.all_to_all(out_rows, 'tp', split_axis=1, concat_axis=0, tiled=True)  13.6 us
    all_gather x1, waiting for transfers between devices, shards(): lax.all_gather(down_part, 'fs', axis=0, tiled=False)  13.6 us
    convert_element_type x2, other arithmetic, shards(): hidden_parts.append((jax.nn.silu(gate_conv) * up_conv).astype(bf16))  10 us
  transfers between devices with their start and end apart: 21, of which 10 were waited for; matrix products, arithmetic and copies ran while one was open for 20% of the time, Pallas kernels for 0%

profile of v1, /device:TPU:0, one launch (start us, length us, event | category | flops | bytes accessed | tf_op | source)
XLA Modules:
  0.0 379.5 jit_solution(8282160342008266549)
XLA Ops:
  6.5 1.9 convert_element_type.145
  8.5 1.2 copy.59
  9.8 1.5 multiply_convert_fusion.7
  11.4 1.1 multiply_convert_fusion.6
  12.6 2.3 fusion.146
  14.9 0.3 copy.85
  15.1 0.3 copy.86
  15.4 0.9 select_convert_fusion
  16.4 0.5 copy.56
  17.0 3.0 collective-permute-start.1
  20.0 2.3 fusion.145
  22.4 0.3 copy.83
  22.6 0.3 copy.84
  22.9 20.4 %collective-permute-done.1 = bf16[1024,512]{0,1:T(8,128)(2,1)} collective-permute-done((bf16[1024,512]{0,1:T(8,128)(2,1)S(1)}, bf16[1024,512]{0,1:T(8,128)(2,1)}, u32[]{:S(2)}, u32[]{:S(2)}) %collective-permute-start.1) | collective-permute-done | bytes 1048608 | tf_op jit(solution)/shard_map/ppermute | solution.py:56
  43.3 0.9 select_convert_fusion.1
  44.4 0.1 fusion.147
  44.7 1.3 constant_dynamic-slice_fusion.23
  45.9 0.3 collective-permute-done.2
  46.3 2.5 fusion
  48.8 3.7 fusion.78
  53.1 3.2 fusion.119
  56.3 0.9 fusion.96
  57.2 1.7 collective-permute-start.4
  58.9 9.7 %all-gather.9.cloned.1.call-done = bf16[256,2048]{0,1:T(8,128)(2,1)} async-done(((bf16[256,512]{0,1:T(8,128)(2,1)}), bf16[256,2048]{0,1:T(8,128)(2,1)}) %all-gather.9.cloned.1.call-update) | async-done | bytes 1048592 | tf_op jit(solution)/shard_map/all_gather | solution.py:135
  68.6 3.7 all-to-all-start
  72.3 0.3 collective-permute-start.3
  72.6 0.3 collective-permute-start.5
  72.9 13.6 %all-to-all-done = bf16[256,4,512]{0,2,1:T(8,128)(2,1)S(1)} async-done(((bf16[256,4,512]{0,2,1:T(8,128)(2,1)}), bf16[256,4,512]{0,2,1:T(8,128)(2,1)S(1)}, u32[]{:S(2)}, u32[]{:S(2)}) %all-to-all-start) | async-done | bytes 1048608 | tf_op jit(solution)/shard_map/all_to_all | solution.py:136
  86.5 0.5 copy.60
  87.2 2.8 add_convert_fusion.4
  90.1 0.4 collective-permute-start.7
  90.7 24.1 %collective-permute-done.7 = bf16[1024,512]{0,1:T(8,128)(2,1)S(1)} collective-permute-done((bf16[1024,512]{0,1:T(8,128)(2,1)S(1)}, bf16[1024,512]{0,1:T(8,128)(2,1)S(1)}, u32[]{:S(2)}, u32[]{:S(2)}) %collective-permute-start.7) | collective-permute-done | bytes 1048608 | tf_op jit(solution)/shard_map/ppermute | solution.py:56
  115.0 0.1 fusion.133
  115.1 13.6 %all-gather.15.cloned.1.call-done = bf16[2816,512]{1,0:T(8,128)(2,1)} async-done(((bf16[704,512]{1,0:T(8,128)(2,1)}), bf16[2816,512]{1,0:T(8,128)(2,1)}) %all-gather.15.cloned.1.call-update) | async-done | bytes 2883600 | tf_op jit(solution)/shard_map/all_gather | solution.py:152
  128.7 1.5 collective-permute-start.11
  130.2 57.8 %all-gather.13.cloned.1.call-done = bf16[2048,704]{0,1:T(8,128)(2,1)} async-done(((bf16[512,704]{0,1:T(8,128)(2,1)}), bf16[2048,704]{0,1:T(8,128)(2,1)}) %all-gather.13.cloned.1.call-update) | async-done | bytes 2883600 | tf_op jit(solution)/shard_map/all_gather | solution.py:151
  188.0 1.5 collective-permute-start.10
  189.4 57.8 %all-gather.11.cloned.1.call-done = bf16[2048,704]{0,1:T(8,128)(2,1)} async-done(((bf16[512,704]{0,1:T(8,128)(2,1)}), bf16[2048,704]{0,1:T(8,128)(2,1)}) %all-gather.11.cloned.1.call-update) | async-done | bytes 2883600 | tf_op jit(solution)/shard_map/all_gather | solution.py:150
  247.2 1.5 collective-permute-start.9
  248.7 2.0 constant_dynamic-slice_fusion.11
  250.7 0.4 constant_dynamic-slice_fusion.15
  251.0 2.1 fusion.3
  253.1 4.5 %fusion.61 = f32[1024,704]{0,1:T(8,128)S(1)} fusion(bf16[512,704]{0,1:T(8,128)(2,1)S(1)} %get-tuple-element.36, bf16[512,704]{0,1:T(8,128)(2,1)S(1)} %get-tuple-element.37, bf16[512,704]{0,1:T(8,128)(2,1)S(1)} %get-tuple-element.38, bf16[512,704]{0,1:T(8,128)(2,1)S(1)} %get-tuple-element.35, f32[704]{0:T(1024)S(1)} %get-tuple-element.86, ...), kind=kOutput, calls=%fused_computation.67 | convolution fusion | flops 2989555712 | bytes 9976576 | tf_op jit(solution)/shard_map/dot_general | solution.py:44
  257.6 4.5 %fusion.58 = f32[1024,704]{0,1:T(8,128)S(1)} fusion(bf16[512,704]{0,1:T(8,128)(2,1)S(1)} %get-tuple-element.30, bf16[512,704]{0,1:T(8,128)(2,1)S(1)} %get-tuple-element.31, bf16[512,704]{0,1:T(8,128)(2,1)S(1)} %get-tuple-element.32, bf16[512,704]{0,1:T(8,128)(2,1)S(1)} %get-tuple-element.29, f32[704]{0:T(1024)S(1)} %get-tuple-element.18, ...), kind=kOutput, calls=%fused_computation.66 | convolution fusion | flops 2989555712 | bytes 9976576 | tf_op jit(solution)/shard_map/dot_general | solution.py:44
  262.1 5.0 %multiply_convert_fusion.3 = bf16[1024,704]{0,1:T(8,128)(2,1)S(1)} fusion(f32[1022,704]{0,1:T(8,128)S(1)} %bitcast.99, f32[1023,704]{0,1:T(8,128)S(1)} %bitcast.100, f32[1024,704]{0,1:T(8,128)S(1)} %fusion.61, f32[1022,704]{0,1:T(8,128)S(1)} %bitcast.103, f32[1023,704]{0,1:T(8,128)S(1)} %bitcast.104, f32[1024,704]{0,1:T(8,128)S(1)} %fusion.58, ...), kind=kLoop, calls=%fused_computation.50 | loop fusion | flops 11534336 | bytes 18743296 | tf_op jit(solution)/shard_map/convert_element_type | solution.py:184
  267.1 1.0 fusion.105
  268.1 48.4 %collective-permute-done.9 = bf16[2048,704]{0,1:T(8,128)(2,1)S(1)} collective-permute-done((bf16[2048,704]{0,1:T(8,128)(2,1)}, bf16[2048,704]{0,1:T(8,128)(2,1)S(1)}, u32[]{:S(2)}, u32[]{:S(2)}) %collective-permute-start.9) | collective-permute-done | bytes 2883616 | tf_op jit(solution)/shard_map/ppermute | solution.py:141
  316.6 2.4 constant_dynamic-slice_fusion.3
  319.0 4.5 %fusion.67 = f32[1024,704]{0,1:T(8,128)S(1)} fusion(bf16[512,704]{0,1:T(8,128)(2,1)S(1)} %get-tuple-element.26, bf16[512,704]{0,1:T(8,128)(2,1)S(1)} %get-tuple-element.27, bf16[512,704]{0,1:T(8,128)(2,1)S(1)} %get-tuple-element.28, bf16[512,704]{0,1:T(8,128)(2,1)S(1)} %get-tuple-element.25, f32[704]{0:T(1024)S(1)} %get-tuple-element.87, ...), kind=kOutput, calls=%fused_computation.69 | convolution fusion | flops 2989555712 | bytes 9976576 | tf_op jit(solution)/shard_map/dot_general | solution.py:44
  323.4 4.5 %fusion.64 = f32[1024,704]{0,1:T(8,128)S(1)} fusion(bf16[512,704]{0,1:T(8,128)(2,1)S(1)} %get-tuple-element.78, bf16[512,704]{0,1:T(8,128)(2,1)S(1)} %get-tuple-element.77, bf16[512,704]{0,1:T(8,128)(2,1)S(1)} %get-tuple-element.76, bf16[512,704]{0,1:T(8,128)(2,1)S(1)} %get-tuple-element.79, f32[704]{0:T(1024)S(1)} %get-tuple-element.17, ...), kind=kOutput, calls=%fused_computation.68 | convolution fusion | flops 2989555712 | bytes 9976576 | tf_op jit(solution)/shard_map/dot_general | solution.py:44
  327.9 5.0 %multiply_convert_fusion = bf16[1024,704]{0,1:T(8,128)(2,1)S(1)} fusion(f32[1022,704]{0,1:T(8,128)S(1)} %bitcast.97, f32[1023,704]{0,1:T(8,128)S(1)} %bitcast.98, f32[1024,704]{0,1:T(8,128)S(1)} %fusion.67, f32[1022,704]{0,1:T(8,128)S(1)} %bitcast.101, f32[1023,704]{0,1:T(8,128)S(1)} %bitcast.102, f32[1024,704]{0,1:T(8,128)S(1)} %fusion.64, ...), kind=kLoop, calls=%fused_computation.47 | loop fusion | flops 11534336 | bytes 18743296 | tf_op jit(solution)/shard_map/convert_element_type | solution.py:184
  333.0 2.7 add_convert_fusion.3
  335.7 1.0 fusion.98
  336.8 1.0 fusion.109
  337.8 3.1 add_convert_fusion.1
  340.9 0.5 collective-permute-start.14
  341.4 2.1 fusion.107
  343.6 0.6 add_convert_fusion.2
  344.3 1.5 collective-permute-start.13
  345.8 2.7 fusion.102
  348.5 2.1 fusion.100
  350.6 18.9 %collective-permute-done.13 = bf16[1024,512]{0,1:T(8,128)(2,1)} collective-permute-done((bf16[1024,512]{0,1:T(8,128)(2,1)S(1)}, bf16[1024,512]{0,1:T(8,128)(2,1)}, u32[]{:S(2)}, u32[]{:S(2)}) %collective-permute-start.13) | collective-permute-done | bytes 1048608 | tf_op jit(solution)/shard_map/ppermute | solution.py:56
  369.5 2.1 fusion.81
  371.6 1.3 copy.73
  (84 shorter events, 1.6 us)
Async XLA Ops:
  6.5 46.5 %copy-start = (bf16[2,128,128]{2,1,0:T(8,128)(2,1)S(1)}, bf16[2,128,128]{2,1,0:T(8,128)(2,1)}, u32[]{:S(2)}) copy-start(bf16[2,128,128]{2,1,0:T(8,128)(2,1)} %param.21) | copy-start | bytes 196612
  6.5 4.9 %copy-start.7 = (f32[1408,512]{1,0:T(8,128)S(1)}, f32[1408,512]{1,0:T(8,128)}, u32[]{:S(2)}) copy-start(f32[1408,512]{1,0:T(8,128)} %param.32) | copy-start | bytes 8650756
  6.5 4.9 %copy-start.14 = (f32[1,512]{1,0:T(1,128)S(1)}, f32[1,512]{1,0:T(1,128)}, u32[]{:S(2)}) copy-start(f32[1,512]{1,0:T(1,128)} %param.33) | copy-start | bytes 6148
  6.5 38.1 %all-gather.7.cloned.1.call-start = ((), (), s32[]{:S(2)}) async-start(), calls=%async_computation.1 | async-start | bytes 1310720 | tf_op jit(solution)/shard_map/all_gather | solution.py:134
  8.5 60.1 %all-gather.9.cloned.1.call-start = ((), (), s32[]{:S(2)}) async-start(), calls=%async_computation.2 | async-start | bytes 1310720 | tf_op jit(solution)/shard_map/all_gather | solution.py:135
  11.3 117.4 %all-gather.15.cloned.1.call-start = ((), (), s32[]{:S(2)}) async-start(), calls=%async_computation.5 | async-start | bytes 3604480 | tf_op jit(solution)/shard_map/all_gather | solution.py:152
  12.5 175.5 %all-gather.13.cloned.1.call-start = ((), (), s32[]{:S(2)}) async-start(), calls=%async_computation.4 | async-start | bytes 3604480 | tf_op jit(solution)/shard_map/all_gather | solution.py:151
  14.9 1.6 copy-start.6
  16.4 230.8 %all-gather.11.cloned.1.call-start = ((), (), s32[]{:S(2)}) async-start(), calls=%async_computation.3 | async-start | bytes 3604480 | tf_op jit(solution)/shard_map/all_gather | solution.py:150
  17.0 26.3 %collective-permute-start.1 = (bf16[1024,512]{0,1:T(8,128)(2,1)S(1)}, bf16[1024,512]{0,1:T(8,128)(2,1)}, u32[]{:S(2)}, u32[]{:S(2)}) collective-permute-start(bf16[1024,512]{0,1:T(8,128)(2,1)S(1)} %bitcast.105), channel_id=1, source_target_pairs={{0,2},{1,3},{2,0},{3,1},{4,6},{5,7},{6,4},{7,5},{8,10},{9,11},{10,... | collective-permute-start | bytes 3145736 | tf_op jit(solution)/shard_map/ppermute | solution.py:56
  20.0 25.9 %collective-permute-start = (bf16[1024,512]{0,1:T(8,128)(2,1)S(1)}, bf16[1024,512]{0,1:T(8,128)(2,1)}, u32[]{:S(2)}, u32[]{:S(2)}) collective-permute-start(bf16[1024,512]{0,1:T(8,128)(2,1)S(1)} %bitcast.106), channel_id=1, source_target_pairs={{0,1},{1,0},{2,3},{3,2},{4,5},{5,4},{6,7},{7,6},{8,9},{9,8},{10,11... | collective-permute-start | bytes 3145736 | tf_op jit(solution)/shard_map/ppermute | solution.py:49
  22.3 22.0 %copy-start.10 = (f32[2048]{0:T(1024)S(1)}, f32[2048]{0:T(1024)}, u32[]{:S(2)}) copy-start(f32[2048]{0:T(1024)} %param.18) | copy-start | bytes 24580
  22.3 22.0 %copy-start.11 = (f32[2048]{0:T(1024)S(1)}, f32[2048]{0:T(1024)}, u32[]{:S(2)}) copy-start(f32[2048]{0:T(1024)} %param.25) | copy-start | bytes 24580
  43.3 3.0 collective-permute-start.2
  44.6 4.1 %copy-start.17 = (f32[1,256]{1,0:T(1,128)S(1)}, f32[1,256]{1,0:T(1,128)}, u32[]{:S(2)}) copy-start(f32[1,256]{1,0:T(1,128)} %param.20) | copy-start | bytes 3076
  53.1 3.2 copy-start.15
  57.2 15.4 %collective-permute-start.4 = (bf16[1024,256]{0,1:T(8,128)(2,1)}, bf16[1024,256]{0,1:T(8,128)(2,1)}, u32[]{:S(2)}, u32[]{:S(2)}) collective-permute-start(bf16[1024,256]{0,1:T(8,128)(2,1)} %fusion.96), channel_id=1, source_target_pairs={{0,2},{1,3},{2,0},{3,1},{4,6},{5,7},{6,4},{7,5},{8,10},{9,11},{10,... | collective-permute-start | bytes 1572872 | tf_op jit(solution)/shard_map/ppermute | solution.py:56
  68.6 17.9 %all-to-all-start = ((bf16[256,4,512]{0,2,1:T(8,128)(2,1)}), bf16[256,4,512]{0,2,1:T(8,128)(2,1)S(1)}, u32[]{:S(2)}, u32[]{:S(2)}) async-start(bf16[256,4,512]{0,2,1:T(8,128)(2,1)} %bitcast.111), calls=%async_computation | async-start | bytes 2097152 | tf_op jit(solution)/shard_map/all_to_all | solution.py:136
  72.3 14.9 %collective-permute-start.3 = (bf16[1024,256]{0,1:T(8,128)(2,1)}, bf16[1024,256]{0,1:T(8,128)(2,1)}, u32[]{:S(2)}, u32[]{:S(2)}) collective-permute-start(bf16[1024,256]{0,1:T(8,128)(2,1)} %fusion.96), channel_id=1, source_target_pairs={{0,1},{1,0},{2,3},{3,2},{4,5},{5,4},{6,7},{7,6},{8,9},{9,8},{10,11... | collective-permute-start | bytes 1572872 | tf_op jit(solution)/shard_map/ppermute | solution.py:49
  72.6 14.6 %collective-permute-start.5 = (bf16[1024,256]{0,1:T(8,128)(2,1)}, bf16[1024,256]{0,1:T(8,128)(2,1)}, u32[]{:S(2)}, u32[]{:S(2)}) collective-permute-start(bf16[1024,256]{0,1:T(8,128)(2,1)} %collective-permute-done.4), channel_id=1, source_target_pairs={{0,1},{1,0},{2,3},{3,2},{4,5},{5,4},{6,7},{7,6},{8,9},{9,8},{10,11... | collective-permute-start | bytes 1572872 | tf_op jit(solution)/shard_map/ppermute | solution.py:49
  87.2 3.3 copy-start.8
  87.2 3.3 copy-start.9
  87.2 27.8 %copy-start.12 = (f32[1,1408]{1,0:T(1,128)S(1)}, f32[1,1408]{1,0:T(1,128)}, u32[]{:S(2)}) copy-start(f32[1,1408]{1,0:T(1,128)} %param.27) | copy-start | bytes 16900
  87.2 27.8 %copy-start.13 = (f32[1,1408]{1,0:T(1,128)S(1)}, f32[1,1408]{1,0:T(1,128)}, u32[]{:S(2)}) copy-start(f32[1,1408]{1,0:T(1,128)} %param.29) | copy-start | bytes 16900
  90.1 24.8 %collective-permute-start.7 = (bf16[1024,512]{0,1:T(8,128)(2,1)S(1)}, bf16[1024,512]{0,1:T(8,128)(2,1)S(1)}, u32[]{:S(2)}, u32[]{:S(2)}) collective-permute-start(bf16[1024,512]{0,1:T(8,128)(2,1)S(1)} %add_convert_fusion.4), channel_id=1, source_target_pairs={{0,2},{1,3},{2,0},{3,1},{4,6},{5,7},{6,4},{7,5},{8,10},{9,11},{10,... | collective-permute-start | bytes 3145736 | tf_op jit(solution)/shard_map/ppermute | solution.py:56
  90.6 160.4 %collective-permute-start.6 = (bf16[1024,512]{0,1:T(8,128)(2,1)S(1)}, bf16[1024,512]{0,1:T(8,128)(2,1)S(1)}, u32[]{:S(2)}, u32[]{:S(2)}) collective-permute-start(bf16[1024,512]{0,1:T(8,128)(2,1)S(1)} %add_convert_fusion.4), channel_id=1, source_target_pairs={{0,1},{1,0},{2,3},{3,2},{4,5},{5,4},{6,7},{7,6},{8,9},{9,8},{10,11... | collective-permute-start | bytes 3145736 | tf_op jit(solution)/shard_map/ppermute | solution.py:49
  114.8 136.2 %collective-permute-start.8 = (bf16[1024,512]{0,1:T(8,128)(2,1)S(1)}, bf16[1024,512]{0,1:T(8,128)(2,1)}, u32[]{:S(2)}, u32[]{:S(2)}) collective-permute-start(bf16[1024,512]{0,1:T(8,128)(2,1)S(1)} %collective-permute-done.7), channel_id=1, source_target_pairs={{0,1},{1,0},{2,3},{3,2},{4,5},{5,4},{6,7},{7,6},{8,9},{9,8},{10,11... | collective-permute-start | bytes 3145736 | tf_op jit(solution)/shard_map/ppermute | solution.py:49
  128.7 204.3 %collective-permute-start.11 = (bf16[4,704,512]{2,1,0:T(8,128)(2,1)}, bf16[4,704,512]{2,1,0:T(8,128)(2,1)}, u32[]{:S(2)}, u32[]{:S(2)}) collective-permute-start(bf16[4,704,512]{2,1,0:T(8,128)(2,1)} %bitcast.115), channel_id=1, source_target_pairs={{0,16},{16,0},{1,17},{17,1},{2,18},{18,2},{3,19},{19,3},{4,20},{20... | collective-permute-start | bytes 8650760 | tf_op jit(solution)/shard_map/ppermute | solution.py:141
  188.0 80.2 %collective-permute-start.10 = (bf16[2048,704]{0,1:T(8,128)(2,1)}, bf16[2048,704]{0,1:T(8,128)(2,1)}, u32[]{:S(2)}, u32[]{:S(2)}) collective-permute-start(bf16[2048,704]{0,1:T(8,128)(2,1)} %all-gather.13.cloned.1.call-done), channel_id=1, source_target_pairs={{0,16},{16,0},{1,17},{17,1},{2,18},{18,2},{3,19},{19,3},{4,20},{20... | collective-permute-start | bytes 8650760 | tf_op jit(solution)/shard_map/ppermute | solution.py:141
  247.2 3.4 copy-start.2
  247.2 69.4 %collective-permute-start.9 = (bf16[2048,704]{0,1:T(8,128)(2,1)}, bf16[2048,704]{0,1:T(8,128)(2,1)S(1)}, u32[]{:S(2)}, u32[]{:S(2)}) collective-permute-start(bf16[2048,704]{0,1:T(8,128)(2,1)} %all-gather.11.cloned.1.call-done), channel_id=1, source_target_pairs={{0,16},{16,0},{1,17},{17,1},{2,18},{18,2},{3,19},{19,3},{4,20},{20... | collective-permute-start | bytes 8650760 | tf_op jit(solution)/shard_map/ppermute | solution.py:141
  262.1 5.0 %copy-start.16 = (bf16[2816,512]{1,0:T(8,128)(2,1)S(1)}, bf16[2816,512]{1,0:T(8,128)(2,1)}, u32[]{:S(2)}) copy-start(bf16[2816,512]{1,0:T(8,128)(2,1)} %all-gather.15.cloned.1.call-done) | copy-start | bytes 8650756
  267.1 69.7 %copy-start.3 = (bf16[1024,704]{0,1:T(8,128)(2,1)}, bf16[1024,704]{0,1:T(8,128)(2,1)S(1)}, u32[]{:S(2)}) copy-start(bf16[1024,704]{0,1:T(8,128)(2,1)S(1)} %multiply_convert_fusion.3) | copy-start | bytes 4325380
  332.9 8.5 %copy-start.4 = (bf16[1024,704]{0,1:T(8,128)(2,1)}, bf16[1024,704]{0,1:T(8,128)(2,1)S(1)}, u32[]{:S(2)}) copy-start(bf16[1024,704]{0,1:T(8,128)(2,1)S(1)} %multiply_convert_fusion) | copy-start | bytes 4325380
  335.6 8.0 %collective-permute-start.12 = (bf16[1024,512]{0,1:T(8,128)(2,1)S(1)}, bf16[1024,512]{0,1:T(8,128)(2,1)S(1)}, u32[]{:S(2)}, u32[]{:S(2)}) collective-permute-start(bf16[1024,512]{0,1:T(8,128)(2,1)S(1)} %add_convert_fusion.3), channel_id=1, source_target_pairs={{0,1},{1,0},{2,3},{3,2},{4,5},{5,4},{6,7},{7,6},{8,9},{9,8},{10,11... | collective-permute-start | bytes 3145736 | tf_op jit(solution)/shard_map/ppermute | solution.py:49
  340.9 9.7 %collective-permute-start.14 = (bf16[1024,512]{0,1:T(8,128)(2,1)}, bf16[1024,512]{0,1:T(8,128)(2,1)S(1)}, u32[]{:S(2)}, u32[]{:S(2)}) collective-permute-start(bf16[1024,512]{0,1:T(8,128)(2,1)} %add_convert_fusion.1), channel_id=1, source_target_pairs={{0,1},{1,0},{2,3},{3,2},{4,5},{5,4},{6,7},{7,6},{8,9},{9,8},{10,11... | collective-permute-start | bytes 3145736 | tf_op jit(solution)/shard_map/ppermute | solution.py:49
  344.3 25.2 %collective-permute-start.13 = (bf16[1024,512]{0,1:T(8,128)(2,1)S(1)}, bf16[1024,512]{0,1:T(8,128)(2,1)}, u32[]{:S(2)}, u32[]{:S(2)}) collective-permute-start(bf16[1024,512]{0,1:T(8,128)(2,1)S(1)} %add_convert_fusion.2), channel_id=1, source_target_pairs={{0,2},{1,3},{2,0},{3,1},{4,6},{5,7},{6,4},{7,5},{8,10},{9,11},{10,... | collective-permute-start | bytes 3145736 | tf_op jit(solution)/shard_map/ppermute | solution.py:56
  345.8 2.7 copy-start.5
  369.5 3.5 copy-start.1
Sparse Core Ops, SparseCore 0:
  8.9 30.6 all-gather.6
  41.2 27.3 all-gather.8
  70.2 58.4 all-gather.14
  130.1 57.7 all-gather.12
  189.4 57.7 all-gather.10
